TPU v7x, 256 devices: a whole 4x4x8 slice. The times are simulated.
256 devices in a mesh: st: 64 (over z, y, core), tp: 4 (over x).
Axes of the slice: x: 4, y: 4, z: 8, core: 2. Of those that a mesh axis runs over, the one named last changes fastest.
Arguments:
- queries: bfloat16 [65536, 1024], P('st', 'tp'), may hold values from -540 to 540
- gate_pre: bfloat16 [65536, 1024], P('st', 'tp'), may hold values from -6 to 6
- cotangent: bfloat16 [65536, 1024], P('st', 'tp'), may hold values from -6 to 6
- store: bfloat16 [81920, 2048], P('st'), may hold values from -6 to 6
- store_gain: float32 [2048], replicated, may hold values from 0.1 to 1.9
- w_key: bfloat16 [2048, 1024], P(None, 'tp'), may hold values from -0.125 to 0.125
- w_value: bfloat16 [2048, 1024], P(None, 'tp'), may hold values from -0.125 to 0.125
- owners: int32 [512, 4], P('st'), may hold values from 0 to 63, all different within a row; in each aligned block of 8 rows (0 to 7, 8 to 15, ...) at most 1 rows name the same one
- slots: int32 [512, 4], P('st'), may hold values from 0 to 19
Outputs:
- grad_queries: float32 [65536, 1024], P('st', 'tp')
- grad_store: float32 [81920, 2048], P(('st', 'tp'))
- grad_w_value: float32 [2048, 1024], P('st', 'tp')
Inputs may be any that keep to these rules, and one draw needn't show every extreme that they name: Each block names 4 different owners. Among the blocks of one device no owner is named twice.
All inputs are finite; a program needn't handle non-finite values.
Results may differ from a plain program's by a relative error of at most 0.014.
Values may be sent and summed in bfloat16 or wider, within the bound.
A program may use at most 192 MiB of HBM per device.

v0:
```python
import jax
import jax.numpy as jnp
from jax import lax
from jax.sharding import Mesh
from jax.sharding import PartitionSpec as P

HD = 128
PLEN = 64
ST = ("st_0", "st_1", "st_2")
ST_TP = ("st_0", "st_1", "st_2", "tp")


EPS = 1e-06


def cut_along(value, dim, size):
    shape = value.shape
    blocks = value.reshape(*shape[:dim], size, shape[dim] // size, *shape[dim + 1 :])
    return jnp.moveaxis(blocks, dim, 0)


def laid_out(blocks, dim):
    shape = list(blocks.shape[1:])
    shape[dim] *= blocks.shape[0]
    return jnp.moveaxis(blocks, 0, dim).reshape(shape)


def turned_blocks(blocks, axes, turns):
    shape = [lax.axis_size(a) for a in axes]
    blocks = blocks.reshape(*shape, *blocks.shape[1:])
    for k in turns:
        blocks = lax.all_to_all(blocks, axes[k], split_axis=k, concat_axis=k, tiled=True)
    return blocks.reshape(-1, *blocks.shape[len(axes) :])


def two_step_exchange(value, groups, turns, split_dim, concat_dim):
    size = lax.axis_size(groups[0]) * lax.axis_size(groups[1])
    blocks = cut_along(value, split_dim, size)
    return laid_out(turned_blocks(blocks, groups, turns), concat_dim)


def sum_at_owner(value, axis, dim):
    blocks = cut_along(value, dim, lax.axis_size(axis))
    arrived = lax.all_to_all(blocks, axis, split_axis=0, concat_axis=0, tiled=True)
    return arrived.sum(axis=0)


def in_one_piece(arrays, axis, dim, along):
    both = jnp.concatenate(arrays, axis=along)
    out, at, outs = (lax.all_gather(both, axis, axis=dim, tiled=True), 0, [])
    for a in arrays:
        outs.append(lax.slice_in_dim(out, at, at + a.shape[along], axis=along))
        at += a.shape[along]
    return tuple(outs)


def row_scale(store_rows):
    return lax.rsqrt(jnp.mean(store_rows * store_rows, axis=-1, keepdims=True) + EPS)


def contract(left, right):
    return lax.dot_general(
        left, right, (((1,), (1,)), ((), ())), preferred_element_type=jnp.float32
    )


def local(queries, gate_pre, cotangent, store, store_gain, w_key, w_value, owners, slots):
    st_size = lax.axis_size(ST)
    tp_size = lax.axis_size("tp")
    blocks, per_block = owners.shape
    tok_rows, local_width = queries.shape
    head_dim = HD
    local_heads = local_width // head_dim
    block_len = tok_rows // blocks
    passage_len = PLEN
    rows_dev = store.shape[0]
    passages = rows_dev // passage_len
    slot_count = blocks * per_block
    slot_cap = (2 * slot_count + st_size - 1) // st_size
    store_rows = store.astype(jnp.float32)
    row_inverse = row_scale(store_rows)
    normed = (store_rows * row_inverse * store_gain).astype(jnp.bfloat16)
    key_table = jnp.dot(normed, w_key, preferred_element_type=jnp.float32).astype(jnp.bfloat16)
    value_table = jnp.dot(normed, w_value, preferred_element_type=jnp.float32).astype(jnp.bfloat16)
    key_table = key_table.reshape(passages, passage_len, local_width)
    value_table = value_table.reshape(passages, passage_len, local_width)
    owner_flat = owners.reshape(slot_count)
    slot_flat = slots.reshape(slot_count)
    slot_order = jnp.arange(slot_count, dtype=jnp.int32)
    earlier_same = (owner_flat[:, None] == owner_flat[None, :]) & (
        slot_order[None, :] < slot_order[:, None]
    )
    slot_rank = jnp.sum(earlier_same.astype(jnp.int32), axis=1)
    position = owner_flat * slot_cap + slot_rank
    places = jnp.arange(st_size * slot_cap, dtype=jnp.int32)
    slot_hits = position[:, None] == places[None, :]
    requests = jnp.sum(jnp.where(slot_hits, slot_flat[:, None], 0), axis=0)
    requests = requests.reshape(st_size, slot_cap)
    asked_ids = two_step_exchange(requests, (("st_0", "st_1"), "st_2"), (1, 0), 0, 0)
    asked_flat = asked_ids.reshape(-1)
    shape_out = asked_ids.shape + (passage_len, local_width)
    picked_keys = jnp.take(key_table, asked_flat, axis=0).reshape(shape_out)
    picked_values = jnp.take(value_table, asked_flat, axis=0).reshape(shape_out)
    sent_keys = lax.all_to_all(picked_keys, ST, split_axis=0, concat_axis=0, tiled=True)
    sent_values = lax.all_to_all(picked_values, ST, split_axis=0, concat_axis=0, tiled=True)
    got_keys, got_values, asked_ids = (sent_keys, sent_values, asked_ids)
    span = per_block * passage_len
    mine_keys = jnp.take(
        got_keys.reshape(st_size * slot_cap, passage_len, local_width), position, axis=0
    )
    mine_values = jnp.take(
        got_values.reshape(st_size * slot_cap, passage_len, local_width), position, axis=0
    )
    mine_keys = mine_keys.reshape(blocks, span, local_heads, head_dim)
    mine_values = mine_values.reshape(blocks, span, local_heads, head_dim)
    score_scale = head_dim ** (-0.5)
    query_blocks = queries.reshape(blocks, block_len, local_heads, head_dim)
    gate_open = jax.nn.sigmoid(gate_pre.astype(jnp.float32))
    grad_in = (gate_open * cotangent.astype(jnp.float32)).astype(jnp.bfloat16)
    grad_in = grad_in.reshape(blocks, block_len, local_heads, head_dim)
    scores = (
        jnp.einsum("bqhd,bkhd->bhqk", query_blocks, mine_keys, preferred_element_type=jnp.float32)
        * score_scale
    )
    shifted = scores - jnp.max(scores, axis=-1, keepdims=True)
    weights = jnp.exp(shifted)
    weights = weights / jnp.sum(weights, axis=-1, keepdims=True)
    weights_half = weights.astype(jnp.bfloat16)
    attended = jnp.einsum(
        "bhqk,bkhd->bqhd", weights_half, mine_values, preferred_element_type=jnp.float32
    )
    row_delta = jnp.sum(grad_in.astype(jnp.float32) * attended, axis=-1)
    grad_weights = jnp.einsum(
        "bqhd,bkhd->bhqk", grad_in, mine_values, preferred_element_type=jnp.float32
    )
    grad_scores = weights * (grad_weights - jnp.transpose(row_delta, (0, 2, 1))[..., None])
    grad_half = grad_scores.astype(jnp.bfloat16)
    grad_queries = (
        jnp.einsum("bhqk,bkhd->bqhd", grad_half, mine_keys, preferred_element_type=jnp.float32)
        * score_scale
    )
    grad_queries = grad_queries.reshape(tok_rows, local_width)
    grad_keys = (
        jnp.einsum("bhqk,bqhd->bkhd", grad_half, query_blocks, preferred_element_type=jnp.float32)
        * score_scale
    )
    grad_values = jnp.einsum(
        "bhqk,bqhd->bkhd", weights_half, grad_in, preferred_element_type=jnp.float32
    )
    grad_keys = grad_keys.reshape(slot_count, passage_len, local_width)
    grad_values = grad_values.reshape(slot_count, passage_len, local_width)
    empty_slots = jnp.zeros((st_size * slot_cap, passage_len, local_width), jnp.float32)
    outgoing_keys = empty_slots.at[position].set(grad_keys)
    outgoing_values = empty_slots.at[position].set(grad_values)
    back_keys, back_values = (
        lax.all_to_all(outgoing_keys, ST, split_axis=0, concat_axis=0, tiled=True),
        lax.all_to_all(outgoing_values, ST, split_axis=0, concat_axis=0, tiled=True),
    )
    asked_flat = asked_ids.reshape(-1)
    owner_pick = (asked_flat[None, :] == jnp.arange(passages, dtype=jnp.int32)[:, None]).astype(
        jnp.float32
    )
    passage_keys = jnp.dot(
        owner_pick,
        back_keys.reshape(st_size * slot_cap, passage_len * local_width),
        precision=lax.Precision.HIGHEST,
        preferred_element_type=jnp.float32,
    )
    passage_values = jnp.dot(
        owner_pick,
        back_values.reshape(st_size * slot_cap, passage_len * local_width),
        precision=lax.Precision.HIGHEST,
        preferred_element_type=jnp.float32,
    )
    passage_keys = passage_keys.astype(jnp.bfloat16).reshape(rows_dev, local_width)
    passage_values = passage_values.astype(jnp.bfloat16).reshape(rows_dev, local_width)
    weight_terms = lax.dot_general(
        normed, passage_values, (((0,), (0,)), ((), ())), preferred_element_type=jnp.float32
    )
    grad_w_value = sum_at_owner(weight_terms, ST, 0)
    quarter = rows_dev // tp_size
    whole_key, whole_value = in_one_piece((w_key, w_value), "tp", 1, 0)
    own_keys, own_values = (
        lax.all_to_all(passage_keys, "tp", split_axis=0, concat_axis=1, tiled=True),
        lax.all_to_all(passage_values, "tp", split_axis=0, concat_axis=1, tiled=True),
    )
    grad_normed = contract(own_keys, whole_key) + contract(own_values, whole_value)
    first_row = lax.axis_index("tp") * quarter
    own_rows = lax.dynamic_slice_in_dim(store_rows, first_row, quarter, 0)
    own_inverse = lax.dynamic_slice_in_dim(row_inverse, first_row, quarter, 0)
    unit_rows = own_rows * own_inverse
    grad_unit = grad_normed * store_gain
    grad_store = own_inverse * (
        grad_unit - unit_rows * jnp.mean(grad_unit * unit_rows, axis=-1, keepdims=True)
    )
    return (grad_queries, grad_store, grad_w_value)


def solution(mesh):
    torus = Mesh(mesh.devices.reshape(8, 4, 2, mesh.shape["tp"]), ("st_0", "st_1", "st_2", "tp"))
    return jax.shard_map(
        local,
        mesh=torus,
        in_specs=(
            P(ST, "tp"),
            P(ST, "tp"),
            P(ST, "tp"),
            P(ST, None),
            P(),
            P(None, "tp"),
            P(None, "tp"),
            P(ST, None),
            P(ST, None),
        ),
        out_specs=(P(ST, "tp"), P(ST_TP, None), P(ST, "tp")),
        check_vma=False,
    )
```

profile of v0, /device:TPU:1, one launch (start us, length us, event | category | flops | bytes accessed | tf_op | source)
XLA Modules:
  0.0 490.7 jit_solution(18441211098978030391)
XLA Ops:
  7.2 0.8 copy.75
  8.2 0.8 copy.76
  9.3 6.6 %all_to_all.73 = s32[32,2,1,1]{0,3,2,1:T(1,128)S(1)} all-to-all(s32[32,2,1,1]{0,3,2,1:T(1,128)S(1)} %copy.77), channel_id=1, replica_groups=mesh['st_0'=8,'st_1'=4,'st_2'=2,'tp'=4] {'st_2'}, dimensions={1} | all-to-all | bytes 512 | tf_op jit(solution)/shard_map/all_to_all | solution.py:32
  15.9 0.7 copy.78
  16.6 9.5 %all-to-all-start.1 = ((s32[32,2,1,1]{1,3,2,0:T(1,128)}), s32[32,2,1,1]{1,3,2,0:T(1,128)S(1)}, u32[]{:S(2)}, u32[]{:S(2)}) async-start(s32[32,2,1,1]{1,3,2,0:T(1,128)} %copy.78), calls=%async_computation.1 | async-start | bytes 32768 | tf_op jit(solution)/shard_map/all_to_all | solution.py:32
  26.1 3.7 multiply_reduce_fusion
  30.1 3.0 convolution_convert_fusion.2
  33.2 1.7 convolution_convert_fusion.3
  35.4 0.7 reduce.3
  36.2 0.7 gather_fusion
  36.9 2.0 gather_fusion.2
  38.9 3.3 select_bitcast_fusion
  42.3 60.2 %all_to_all.74 = bf16[64,1,64,256]{3,2,1,0:T(8,128)(2,1)} all-to-all(bf16[64,1,64,256]{3,2,1,0:T(8,128)(2,1)S(1)} %get-tuple-element.18), channel_id=1, replica_groups=mesh['st_0'=8,'st_1'=4,'st_2'=2,'tp'=4] {'st_0','st_1','st_2'}, dimensions={0} | all-to-all | bytes 4194304 | tf_op jit(solution)/shard_map/all_to_all | solution.py:105
  102.5 7.6 %all-to-all-start.2 = ((bf16[64,1,64,256]{3,2,1,0:T(8,128)(2,1)}), bf16[64,1,64,256]{3,2,1,0:T(8,128)(2,1)}, u32[]{:S(2)}, u32[]{:S(2)}) async-start(bf16[64,1,64,256]{3,2,1,0:T(8,128)(2,1)} %get-tuple-element.19), calls=%async_computation.2 | async-start | bytes 4194304 | tf_op jit(solution)/shard_map/all_to_all | solution.py:104
  110.8 1.1 copy.84
  111.9 2.2 gather_fusion.3
  114.1 45.4 %all-to-all-done.2 = bf16[64,1,64,256]{3,2,1,0:T(8,128)(2,1)} async-done(((bf16[64,1,64,256]{3,2,1,0:T(8,128)(2,1)}), bf16[64,1,64,256]{3,2,1,0:T(8,128)(2,1)}, u32[]{:S(2)}, u32[]{:S(2)}) %all-to-all-start.2) | async-done | bytes 2097184 | tf_op jit(solution)/shard_map/all_to_all | solution.py:104
  159.5 2.2 gather_fusion.1
  161.7 1.6 broadcast_select_fusion
  163.3 1.3 reshape.147
  164.7 0.7 copy.88
  165.9 1.6 fusion.32
  167.5 1.3 copy-done.8
  169.3 2.3 copy.97
  171.6 2.9 reshape.205
  174.5 2.5 broadcast_in_dim.52.clone
  177.0 5.4 %scatter_fusion.1 = f32[64,64,256]{2,1,0:T(8,128)} fusion(f32[64,64,256]{2,1,0:T(8,128)} %broadcast_in_dim.52.clone, s32[32]{0:T(128)S(1)} %fusion.27, f32[32,64,256]{2,1,0:T(8,128)S(1)} %reshape.205), kind=kCustom, calls=%fused_computation.5 | custom fusion | bytes 6291584 | tf_op jit(solution)/shard_map/scatter | solution.py:154
  182.4 7.4 %all-to-all-start.6 = ((f32[64,64,256]{2,1,0:T(8,128)}), f32[64,64,256]{2,1,0:T(8,128)}, u32[]{:S(2)}, u32[]{:S(2)}) async-start(f32[64,64,256]{2,1,0:T(8,128)} %scatter_fusion.1), calls=%async_computation.6 | async-start | bytes 8388608 | tf_op jit(solution)/shard_map/all_to_all | solution.py:157
  190.1 0.7 copy.85
  190.8 2.3 fusion.18
  193.9 1.0 copy-done.3
  195.3 2.9 copy.93
  198.2 2.9 reshape.197
  201.2 2.5 broadcast_in_dim.52.clone.1
  203.7 5.4 %scatter_fusion = f32[64,64,256]{2,1,0:T(8,128)} fusion(f32[64,64,256]{2,1,0:T(8,128)} %broadcast_in_dim.52.clone.1, s32[32]{0:T(128)S(1)} %fusion.27, f32[32,64,256]{2,1,0:T(8,128)S(1)} %reshape.197), kind=kCustom, calls=%fused_computation.4 | custom fusion | bytes 6291584 | tf_op jit(solution)/shard_map/scatter | solution.py:153
  209.1 75.4 %all-to-all-done.6 = f32[64,64,256]{2,1,0:T(8,128)} async-done(((f32[64,64,256]{2,1,0:T(8,128)}), f32[64,64,256]{2,1,0:T(8,128)}, u32[]{:S(2)}, u32[]{:S(2)}) %all-to-all-start.6) | async-done | bytes 4194336 | tf_op jit(solution)/shard_map/all_to_all | solution.py:157
  284.6 7.0 %all-to-all-start.4 = ((f32[64,64,256]{2,1,0:T(8,128)}), f32[64,64,256]{2,1,0:T(8,128)}, u32[]{:S(2)}, u32[]{:S(2)}) async-start(f32[64,64,256]{2,1,0:T(8,128)} %scatter_fusion), calls=%async_computation.4 | async-start | bytes 8388608 | tf_op jit(solution)/shard_map/all_to_all | solution.py:156
  291.9 1.5 pad_maximum_fusion
  293.4 4.6 copy.115
  297.9 1.5 convolution_convert_fusion
  299.5 1.3 all_to_all.59
  300.8 85.7 %all-to-all-done.4 = f32[64,64,256]{2,1,0:T(8,128)} async-done(((f32[64,64,256]{2,1,0:T(8,128)}), f32[64,64,256]{2,1,0:T(8,128)}, u32[]{:S(2)}, u32[]{:S(2)}) %all-to-all-start.4) | async-done | bytes 4194336 | tf_op jit(solution)/shard_map/all_to_all | solution.py:156
  386.5 4.0 all-to-all-start.7
  390.5 4.6 copy.114
  395.1 1.5 convolution_convert_fusion.1
  396.6 1.3 all_to_all.54
  397.9 1.0 all-to-all-done.7
  399.0 3.7 all-to-all-start.5
  402.7 6.1 %fusion.31 = bf16[2048,1280]{0,1:T(8,128)(2,1)} fusion(f32[2048]{0:T(1024)S(1)} %copy-done.18, f32[1280]{0:T(1024)S(1)} %add_rsqrt_fusion, bf16[1280,2048]{1,0:T(8,128)(2,1)} %param.16), kind=kLoop, calls=%fused_computation.68 | loop fusion | flops 10485760 | bytes 10499072 | tf_op jit(solution)/shard_map/dot_general | solution.py:177
  408.8 7.9 %copy.99 = bf16[2048,1280]{1,0:T(8,128)(2,1)} copy(bf16[2048,1280]{0,1:T(8,128)(2,1)} %fusion.31) | data formatting | bytes 10485760 | tf_op jit(solution)/shard_map/dot_general | solution.py:177
  417.1 5.3 %fusion.33 = f32[64,32,256]{2,1,0:T(8,128)} fusion(bf16[64,32,1280]{2,1,0:T(8,128)(2,1)} %bitcast.79, bf16[1280,256,1]{1,0,2:T(8,128)(2,1)S(1)} %reshape.221), kind=kOutput, calls=%fused_computation.70 | convolution fusion | flops 1342177280 | bytes 7995392 | tf_op jit(solution)/shard_map/dot_general | solution.py:177
  422.5 0.8 copy-done.6
  423.3 9.6 %all-to-all-start.8 = ((f32[64,32,256]{2,1,0:T(8,128)}), f32[64,32,256]{2,1,0:T(8,128)S(1)}, u32[]{:S(2)}, u32[]{:S(2)}) async-start(f32[64,32,256]{2,1,0:T(8,128)} %fusion.33), calls=%async_computation.8 | async-start | bytes 4194304 | tf_op jit(solution)/shard_map/all_to_all | solution.py:44
  432.9 7.9 %convert_element_type.40 = f32[1280,2048]{1,0:T(8,128)} convert(bf16[1280,2048]{1,0:T(8,128)(2,1)} %param.16) | non-fusion elementwise | flops 2621440 | bytes 15728640 | tf_op jit(solution)/shard_map/convert_element_type | solution.py:80
  440.9 2.6 fusion.16
  443.5 1.6 copy.108
  445.1 1.0 copy.121
  446.2 2.0 copy.112
  448.3 4.1 fusion.1
  452.4 0.7 copy-done.19
  453.1 3.8 multiply_reduce_fusion.1
  456.9 3.7 subtract_multiply_fusion
  460.6 22.0 %all-to-all-done.8 = f32[64,32,256]{2,1,0:T(8,128)S(1)} async-done(((f32[64,32,256]{2,1,0:T(8,128)}), f32[64,32,256]{2,1,0:T(8,128)S(1)}, u32[]{:S(2)}, u32[]{:S(2)}) %all-to-all-start.8) | async-done | bytes 2097184 | tf_op jit(solution)/shard_map/all_to_all | solution.py:44
  482.6 0.8 reduce_sum.72
  (70 shorter events, 5.6 us)
Async XLA Ops:
  16.6 18.3 %all-to-all-start.1 = ((s32[32,2,1,1]{1,3,2,0:T(1,128)}), s32[32,2,1,1]{1,3,2,0:T(1,128)S(1)}, u32[]{:S(2)}, u32[]{:S(2)}) async-start(s32[32,2,1,1]{1,3,2,0:T(1,128)} %copy.78), calls=%async_computation.1 | async-start | bytes 32768 | tf_op jit(solution)/shard_map/all_to_all | solution.py:32
  26.1 4.0 copy-start
  26.1 4.0 copy-start.18
  30.1 3.0 copy-start.11
  102.4 7.7 %copy-start.15 = (bf16[1024,256]{1,0:T(8,128)(2,1)S(1)}, bf16[1024,256]{1,0:T(8,128)(2,1)}, u32[]{:S(2)}) copy-start(bf16[1024,256]{1,0:T(8,128)(2,1)} %param.13) | copy-start | bytes 1572868
  102.4 7.9 %copy-start.13 = (bf16[1024,256]{1,0:T(8,128)(2,1)S(1)}, bf16[1024,256]{1,0:T(8,128)(2,1)}, u32[]{:S(2)}) copy-start(bf16[1024,256]{1,0:T(8,128)(2,1)} %param.15) | copy-start | bytes 1572868
  102.5 7.9 %copy-start.14 = (bf16[1024,256]{1,0:T(8,128)(2,1)S(1)}, bf16[1024,256]{1,0:T(8,128)(2,1)}, u32[]{:S(2)}) copy-start(bf16[1024,256]{1,0:T(8,128)(2,1)} %param.14) | copy-start | bytes 1572868
  102.5 57.1 %all-to-all-start.2 = ((bf16[64,1,64,256]{3,2,1,0:T(8,128)(2,1)}), bf16[64,1,64,256]{3,2,1,0:T(8,128)(2,1)}, u32[]{:S(2)}, u32[]{:S(2)}) async-start(bf16[64,1,64,256]{3,2,1,0:T(8,128)(2,1)} %get-tuple-element.19), calls=%async_computation.2 | async-start | bytes 4194304 | tf_op jit(solution)/shard_map/all_to_all | solution.py:104
  110.3 55.0 %copy-start.1 = (bf16[8,128,2,128]{3,2,1,0:T(2,128)(2,1)}, bf16[8,128,2,128]{3,2,1,0:T(2,128)(2,1)S(1)}, u32[]{:S(2)}) copy-start(bf16[8,128,2,128]{3,2,1,0:T(2,128)(2,1)S(1)} %reshape.148) | copy-start | bytes 1572868
  165.9 3.0 copy-start.16
  167.5 1.3 copy-start.8
  182.4 7.4 %copy-start.4 = (bf16[32,64,256]{2,1,0:T(8,128)(2,1)S(1)}, bf16[32,64,256]{2,1,0:T(8,128)(2,1)}, u32[]{:S(2)}) copy-start(bf16[32,64,256]{2,1,0:T(8,128)(2,1)} %get-tuple-element.16) | copy-start | bytes 3145732
  182.4 102.2 %all-to-all-start.6 = ((f32[64,64,256]{2,1,0:T(8,128)}), f32[64,64,256]{2,1,0:T(8,128)}, u32[]{:S(2)}, u32[]{:S(2)}) async-start(f32[64,64,256]{2,1,0:T(8,128)} %scatter_fusion.1), calls=%async_computation.6 | async-start | bytes 8388608 | tf_op jit(solution)/shard_map/all_to_all | solution.py:157
  190.8 2.4 copy-start.9
  190.8 2.5 copy-start.17
  193.3 1.6 copy-start.2
  193.9 1.0 copy-start.3
  209.1 82.8 %copy-start.10 = (bf16[2048,256]{1,0:T(8,128)(2,1)S(1)}, bf16[2048,256]{1,0:T(8,128)(2,1)}, u32[]{:S(2)}) copy-start(bf16[2048,256]{1,0:T(8,128)(2,1)} %param.19) | copy-start | bytes 3145732
  209.1 82.8 %copy-start.12 = (bf16[2048,256]{1,0:T(8,128)(2,1)S(1)}, bf16[2048,256]{1,0:T(8,128)(2,1)}, u32[]{:S(2)}) copy-start(bf16[2048,256]{1,0:T(8,128)(2,1)} %param.18) | copy-start | bytes 3145732
  284.6 101.9 %all-to-all-start.4 = ((f32[64,64,256]{2,1,0:T(8,128)}), f32[64,64,256]{2,1,0:T(8,128)}, u32[]{:S(2)}, u32[]{:S(2)}) async-start(f32[64,64,256]{2,1,0:T(8,128)} %scatter_fusion), calls=%async_computation.4 | async-start | bytes 8388608 | tf_op jit(solution)/shard_map/all_to_all | solution.py:156
  291.6 156.7 %all-gather.2.cloned.1.call-start = ((), (), s32[]{:S(2)}) async-start(), calls=%async_computation.9 | async-start | bytes 10485760 | tf_op jit(solution)/shard_map/all_gather | solution.py:50
  386.5 12.5 %all-to-all-start.7 = ((bf16[4,320,256]{2,1,0:T(8,128)(2,1)}), bf16[4,320,256]{2,1,0:T(8,128)(2,1)S(1)}, u32[]{:S(2)}, u32[]{:S(2)}) async-start(bf16[4,320,256]{2,1,0:T(8,128)(2,1)} %all_to_all.59), calls=%async_computation.7 | async-start | bytes 1310720 | tf_op jit(solution)/shard_map/all_to_all | solution.py:185
  399.0 9.9 %copy-start.5 = (bf16[4,320,256]{2,1,0:T(8,128)(2,1)}, bf16[4,320,256]{2,1,0:T(8,128)(2,1)S(1)}, u32[]{:S(2)}) copy-start(bf16[4,320,256]{2,1,0:T(8,128)(2,1)S(1)} %all-to-all-done.7) | copy-start | bytes 1966084
  399.0 23.5 %all-to-all-start.5 = ((bf16[4,320,256]{2,1,0:T(8,128)(2,1)}), bf16[4,320,256]{2,1,0:T(8,128)(2,1)S(1)}, u32[]{:S(2)}, u32[]{:S(2)}) async-start(bf16[4,320,256]{2,1,0:T(8,128)(2,1)} %all_to_all.54), calls=%async_computation.5 | async-start | bytes 1310720 | tf_op jit(solution)/shard_map/all_to_all | solution.py:184
  422.5 0.8 copy-start.6
  423.3 59.3 %all-to-all-start.8 = ((f32[64,32,256]{2,1,0:T(8,128)}), f32[64,32,256]{2,1,0:T(8,128)S(1)}, u32[]{:S(2)}, u32[]{:S(2)}) async-start(f32[64,32,256]{2,1,0:T(8,128)} %fusion.33), calls=%async_computation.8 | async-start | bytes 4194304 | tf_op jit(solution)/shard_map/all_to_all | solution.py:44
  445.1 3.1 copy-start.7
  448.3 4.8 copy-start.19
Sparse Core Ops, SparseCore 0:
  294.8 88.6 all-gather.1
where the time goes:
time: 499 us; the launch traced here: 491 us
  waiting for transfers between devices  230 us (46%)
  local copies, waits for them, and re-layouts  70.8 us (14%)
  blocking collectives  66.7 us (13%)
  starting transfers between devices  49.1 us (10%)
  other arithmetic  31.5 us (6%)
  matrix products  27.9 us (6%)
  between operations  14.9 us (3%)
    all_to_all x1, waiting for transfers between devices, local(): lax.all_to_all(outgoing_keys, ST, split_axis=0, concat_axis=0, tiled=True)  85.7 us
    all_to_all x1, waiting for transfers between devices, local(): lax.all_to_all(outgoing_values, ST, split_axis=0, concat_axis=0, tiled=True)  75.4 us
    all_to_all x1, blocking collectives, local(): lax.all_to_all(picked_values, ST, split_axis=0, concat_axis=0, tiled=True)  60.2 us
    all_to_all x1, waiting for transfers between devices, local(): lax.all_to_all(picked_keys, ST, split_axis=0, concat_axis=0, tiled=True)  45.4 us
    all_to_all x1, waiting for transfers between devices, sum_at_owner(): lax.all_to_all(blocks, axis, split_axis=0, concat_axis=0, tiled=True)  22 us
    unnamed x46, local copies, waits for them, and re-layouts  17.6 us
  transfers between devices with their start and end apart: 8, of which 5 were waited for; matrix products, arithmetic and copies ran while one was open for 19% of the time, Pallas kernels for 0%

commit v1 on v0

v1 whole, which is shorter than its diff:
```python
import functools

import jax
import jax.numpy as jnp
from jax import lax
from jax.experimental import pallas as pl
from jax.experimental.pallas import tpu as pltpu
from jax.sharding import Mesh
from jax.sharding import PartitionSpec as P

HD = 128
PLEN = 64
ST = ("st_0", "st_1", "st_2")
ST_TP = ("st_0", "st_1", "st_2", "tp")
MESH = pl.DeviceIdType.MESH
EPS = 1e-06
BF = jnp.bfloat16
F32 = jnp.float32

NN = (((1,), (0,)), ((), ()))
NT = (((1,), (1,)), ((), ()))
TN = (((0,), (0,)), ((), ()))


def dot(a, b, dims=NN):
    return lax.dot_general(a, b, dims, preferred_element_type=F32)


def kernel(
    cfg,
    store_hbm,
    wk_hbm,
    wv_hbm,
    q_hbm,
    gate_hbm,
    cot_hbm,
    gain_ref,
    req_ref,
    pos_ref,
    inv_ref,
    dq_ref,
    gs_ref,
    gw_ref,
    store,
    normed,
    wk_all,
    wv_all,
    q,
    gate,
    gin,
    table,
    snd_a,
    snd_b,
    k_rcv,
    v_rcv,
    dv_rcv,
    dk_snd_0,
    dk_snd_1,
    dk_rcv_0,
    dk_rcv_1,
    wts,
    slot_a,
    run,
    pas_v,
    pas_k,
    own_v,
    own_k,
    gn,
    gw_full,
    gwc_rcv,
    gwy,
    gwy_rcv,
    gwz,
    gwz_rcv,
    asked_v,
    meta_v,
    meta_s,
    load_sem,
    self_sem,
    ssem,
    rsem,
):
    nz, ny, nc, nx, npass = cfg
    nst = nz * ny * nc
    dk_snd = (dk_snd_0, dk_snd_1)
    dk_rcv = (dk_rcv_0, dk_rcv_1)
    rows, width = store.shape
    heads = wk_all.shape[2] // HD
    blocks = q.shape[0] // 128
    per = pos_ref.shape[0] // blocks
    quarter = rows // nx
    z = lax.axis_index("st_0")
    y = lax.axis_index("st_1")
    c = lax.axis_index("st_2")
    x = lax.axis_index("tp")
    me = (z * ny + y) * nc + c
    WV, REQ, K, V, DV, DK, WK, XV, XK, GC, GY, GZ = 0, 1, 2, 3, 4, 5, 7, 8, 9, 11, 12, 13

    def st_peer(i):
        pz = lax.rem(z + i // (ny * nc), nz)
        py = lax.rem(y + lax.rem(i // nc, ny), ny)
        pc = lax.rem(c + lax.rem(i, nc), nc)
        return (pz, py, pc, x), (pz * ny + py) * nc + pc

    def x_peer(i):
        px = lax.rem(x + i, nx)
        return (z, y, c, px), px

    barrier = pltpu.get_barrier_semaphore()

    @pl.loop(1, nst)
    def _(i):
        pl.semaphore_signal(barrier, inc=1, device_id=st_peer(i)[0], device_id_type=MESH)

    @pl.loop(1, nx)
    def _(i):
        pl.semaphore_signal(barrier, inc=1, device_id=x_peer(i)[0], device_id_type=MESH)

    chunk = rows // 5
    loads = [
        pltpu.make_async_copy(
            store_hbm.at[pl.ds(i * chunk, chunk)], store.at[pl.ds(i * chunk, chunk)], load_sem.at[i]
        )
        for i in range(5)
    ]
    load_k = pltpu.make_async_copy(wk_hbm, wk_all.at[x], load_sem.at[5])
    load_v = pltpu.make_async_copy(wv_hbm, wv_all.at[x], load_sem.at[6])
    load_q = pltpu.make_async_copy(q_hbm, q, load_sem.at[7])
    load_g = pltpu.make_async_copy(gate_hbm, gate, load_sem.at[8])
    load_c = pltpu.make_async_copy(cot_hbm, gin, load_sem.at[9])
    load_k.start()
    for cp in loads:
        cp.start()
    load_v.start()
    load_q.start()
    load_g.start()
    load_c.start()
    pl.semaphore_wait(barrier, nst + nx - 2)

    def send_st(src, dst, k):
        @pl.loop(1, nst)
        def _(i):
            device, t = st_peer(i)
            pltpu.make_async_remote_copy(
                src_ref=src.at[t],
                dst_ref=dst.at[me],
                send_sem=ssem.at[k],
                recv_sem=rsem.at[k],
                device_id=device,
                device_id_type=MESH,
            ).start()

        own = pltpu.make_async_copy(src.at[me], dst.at[me], self_sem.at[k])
        own.start()
        return own

    def bulk_wait(buf, n, sem):
        part = buf.at[pl.ds(0, n)]
        pltpu.make_async_copy(part, part, sem).wait()

    own_req = send_st(req_ref, asked_v, REQ)

    load_k.wait()
    for i in range(5):
        loads[i].wait()

        @pl.loop(0, chunk // 64)
        def _(j):
            at = pl.ds(pl.multiple_of(i * chunk + j * 64, 64), 64)
            s = store[at, :].astype(F32)
            r = lax.rsqrt(jnp.mean(s * s, axis=-1, keepdims=True) + EPS)
            normed[at, :] = (s * r * gain_ref[...]).astype(BF)

        at = pl.ds(i * chunk, chunk)
        part = pl.ds(i * (chunk // PLEN), chunk // PLEN)
        keys = dot(normed[at, :], wk_all[x]).astype(BF)
        table[part] = keys.reshape(chunk // PLEN, PLEN, heads * HD)

    own_req.wait()
    bulk_wait(asked_v, nst - 1, rsem.at[REQ])
    asked = asked_v[...].reshape(nst, 128)
    lane = lax.broadcasted_iota(jnp.int32, (nst, 128), 1)
    row = lax.broadcasted_iota(jnp.int32, (nst, 128), 0)
    slot_col = jnp.where(asked < 0, npass, asked)
    key_col = slot_col * nst + row
    diag = lane == row
    key_row = jnp.sum(jnp.where(diag, key_col, 0), axis=0, keepdims=True)
    below = (lane < nst) & (key_row < key_col)
    rank = jnp.sum(below.astype(jnp.int32), axis=1, keepdims=True)
    order_row = jnp.sum(jnp.where(rank == lane, row, 0), axis=0, keepdims=True)
    sorted_row = jnp.sum(jnp.where(rank == lane, slot_col, 0), axis=0, keepdims=True)
    keep_row = jnp.sum(
        jnp.where((rank == lane - 1) & (slot_col == sorted_row), 1, 0), axis=0, keepdims=True
    )
    last_row = jnp.sum((slot_col <= lane).astype(jnp.int32), axis=0, keepdims=True) - 1
    count_row = jnp.sum((slot_col == lane).astype(jnp.int32), axis=0, keepdims=True)
    pick_row = jnp.sum(jnp.where(diag, jnp.maximum(asked, 0), 0), axis=0, keepdims=True)
    meta_v[0:1, :] = pick_row
    meta_v[1:2, :] = order_row
    meta_v[2:3, :] = keep_row
    meta_v[3:4, :] = jnp.maximum(last_row, 0)
    meta_v[4:5, :] = jnp.minimum(count_row, 1)
    to_s = pltpu.make_async_copy(meta_v, meta_s, load_sem.at[10])
    to_s.start()
    to_s.wait()

    def gather(src, dst):
        @pl.loop(0, nst)
        def _(t):
            dst[t] = src[meta_s[0, t]]

    gather(table, snd_a)
    own_k_copy = send_st(snd_a, k_rcv, K)

    load_v.wait()
    for i in range(5):
        at = pl.ds(i * chunk, chunk)
        part = pl.ds(i * (chunk // PLEN), chunk // PLEN)
        values = dot(normed[at, :], wv_all[x]).astype(BF)
        table[part] = values.reshape(chunk // PLEN, PLEN, heads * HD)
    gather(table, snd_b)
    own_v_copy = send_st(snd_b, v_rcv, V)

    for w_all, k in ((wk_all, WK), (wv_all, WV)):

        @pl.loop(1, nx)
        def _(i):
            device, _px = x_peer(i)
            pltpu.make_async_remote_copy(
                src_ref=w_all.at[x],
                dst_ref=w_all.at[x],
                send_sem=ssem.at[k],
                recv_sem=rsem.at[k],
                device_id=device,
                device_id_type=MESH,
            ).start()

    load_q.wait()
    load_g.wait()
    load_c.wait()

    @pl.loop(0, blocks)
    def _(b):
        at = pl.ds(pl.multiple_of(b * 128, 128), 128)
        opened = jax.nn.sigmoid(gate[at, :].astype(F32))
        gin[at, :] = (opened * gin[at, :].astype(F32)).astype(BF)

    scale = HD ** (-0.5)

    def passages(ref, b, h):
        parts = [ref[pos_ref[b * per + j], :, h * HD : (h + 1) * HD] for j in range(per)]
        return jnp.concatenate(parts, axis=0)

    own_k_copy.wait()
    bulk_wait(k_rcv, nst - 1, rsem.at[K])

    @pl.loop(0, blocks)
    def _(b):
        at = pl.ds(pl.multiple_of(b * 128, 128), 128)
        for h in range(heads):
            cols = slice(h * HD, (h + 1) * HD)
            kh = passages(k_rcv, b, h)
            s = dot(kh, q[at, cols], NT) * scale
            e = jnp.exp(s - jnp.max(s, axis=0, keepdims=True))
            w = e / jnp.sum(e, axis=0, keepdims=True)
            wts[b * heads + h] = w
            dv = dot(w.astype(BF), gin[at, cols]).astype(BF)
            for j in range(per):
                slot_a[b * per + j, :, cols] = dv[j * PLEN : (j + 1) * PLEN]

    bulk_wait(snd_a, nst - 1, ssem.at[K])

    @pl.loop(0, nst)
    def _(t):
        snd_a[t] = slot_a[inv_ref[t]]

    own_dv_copy = send_st(snd_a, dv_rcv, DV)

    own_v_copy.wait()
    bulk_wait(v_rcv, nst - 1, rsem.at[V])

    for h in range(heads):
        cols = slice(h * HD, (h + 1) * HD)

        @pl.loop(0, blocks)
        def _(b):
            at = pl.ds(pl.multiple_of(b * 128, 128), 128)
            kh = passages(k_rcv, b, h)
            vh = passages(v_rcv, b, h)
            gwt = dot(vh, gin[at, cols], NT)
            w = wts[b * heads + h]
            delta = jnp.sum(w.astype(BF).astype(F32) * gwt, axis=0, keepdims=True)
            gsc = (w * (gwt - delta)).astype(BF)
            dk = (dot(gsc, q[at, cols]) * scale).astype(BF)
            for j in range(per):
                slot_a[b * per + j, :, cols] = dk[j * PLEN : (j + 1) * PLEN]
            dq_ref[at, cols] = dot(gsc, kh, TN) * scale

        @pl.loop(0, nst)
        def _(t):
            dk_snd[h][t] = slot_a[inv_ref[t], :, cols]

        send_st(dk_snd[h], dk_rcv[h], DK + h)

    def owner_sum(rcv, cols, out):
        def step(i, acc):
            acc = acc * meta_s[2, i].astype(F32) + rcv[meta_s[1, i]].astype(F32)
            run[i, :, cols] = acc.astype(BF)
            return acc

        wide = cols.stop - cols.start
        lax.fori_loop(0, nst, step, jnp.zeros((PLEN, wide), F32))

        @pl.loop(0, npass)
        def _(p):
            got = run[meta_s[3, p], :, cols].astype(F32)
            some = meta_s[4, p].astype(F32)
            out[pl.ds(pl.multiple_of(p * PLEN, PLEN), PLEN), :] = (got * some).astype(BF)

    def send_x(src, dst, k):
        @pl.loop(1, nx)
        def _(i):
            device, px = x_peer(i)
            pltpu.make_async_remote_copy(
                src_ref=src.at[pl.ds(pl.multiple_of(px * quarter, 64), quarter)],
                dst_ref=dst.at[x],
                send_sem=ssem.at[k],
                recv_sem=rsem.at[k],
                device_id=device,
                device_id_type=MESH,
            ).start()

        own = pltpu.make_async_copy(
            src.at[pl.ds(pl.multiple_of(x * quarter, 64), quarter)], dst.at[x], self_sem.at[k]
        )
        own.start()
        return own

    own_dv_copy.wait()
    bulk_wait(dv_rcv, nst - 1, rsem.at[DV])
    owner_sum(dv_rcv, slice(0, heads * HD), pas_v)
    own_xv = send_x(pas_v, own_v, XV)

    tile = 256
    pv_t = pas_v[...].T

    @pl.loop(0, width // tile)
    def _(j):
        at = pl.multiple_of(j * tile, tile)
        part = dot(pv_t, normed[:, pl.ds(at, tile)]).T
        gw_full[pl.ds(j * (tile // gw_full.shape[1]), tile // gw_full.shape[1])] = part.reshape(
            tile // gw_full.shape[1], gw_full.shape[1], heads * HD
        )

    other = lax.rem(c + 1, nc)
    gw_by = gw_full.reshape(nz * ny, nc, gw_full.shape[1], heads * HD)
    to_core = pltpu.make_async_remote_copy(
        src_ref=gw_by.at[:, other],
        dst_ref=gwc_rcv,
        send_sem=ssem.at[GC],
        recv_sem=rsem.at[GC],
        device_id=(z, y, other, x),
        device_id_type=MESH,
    )
    to_core.start()

    bulk_wait(wk_all, nx - 1, rsem.at[WK])
    bulk_wait(wv_all, nx - 1, rsem.at[WV])
    own_xv.wait()
    bulk_wait(own_v, nx - 1, rsem.at[XV])

    @pl.loop(0, width // tile)
    def _(j):
        at = pl.ds(pl.multiple_of(j * tile, tile), tile)
        acc = dot(own_v[0], wv_all[0, at, :], NT)
        for s in range(1, nx):
            acc += dot(own_v[s], wv_all[s, at, :], NT)
        gn[:, at] = acc

    to_core.wait()

    @pl.loop(0, nz * ny)
    def _(i):
        zi, yi = i // ny, lax.rem(i, ny)
        gwy[yi, zi] = gw_full[i * nc + c] + gwc_rcv[i]

    @pl.loop(1, ny)
    def _(i):
        py = lax.rem(y + i, ny)
        pltpu.make_async_remote_copy(
            src_ref=gwy.at[py],
            dst_ref=gwy_rcv.at[i],
            send_sem=ssem.at[GY],
            recv_sem=rsem.at[GY],
            device_id=(z, py, c, x),
            device_id_type=MESH,
        ).start()

    bulk_wait(gwy, ny - 1, ssem.at[GY])
    bulk_wait(gwy_rcv, ny - 1, rsem.at[GY])

    @pl.loop(0, nz)
    def _(i):
        acc = gwy[y, i]
        for j in range(1, ny):
            acc += gwy_rcv[j, i]
        gwz[i] = acc

    @pl.loop(1, nz)
    def _(i):
        pz = lax.rem(z + i, nz)
        pltpu.make_async_remote_copy(
            src_ref=gwz.at[pz],
            dst_ref=gwz_rcv.at[i],
            send_sem=ssem.at[GZ],
            recv_sem=rsem.at[GZ],
            device_id=(pz, y, c, x),
            device_id_type=MESH,
        ).start()

    def keys_half(h):
        own = pltpu.make_async_copy(dk_snd[h].at[me], dk_rcv[h].at[me], self_sem.at[DK + h])
        own.wait()
        bulk_wait(dk_rcv[h], nst - 1, rsem.at[DK + h])
        owner_sum(dk_rcv[h], slice(0, HD), pas_k.at[h])
        own_x = send_x(pas_k.at[h], own_k.at[h], XK + h)
        own_x.wait()
        bulk_wait(own_k.at[h], nx - 1, rsem.at[XK + h])

        @pl.loop(0, width // tile)
        def _(j):
            at = pl.ds(pl.multiple_of(j * tile, tile), tile)
            acc = gn[:, at]
            for s in range(nx):
                acc += dot(own_k[h, s], wk_all[s, at, h * HD : (h + 1) * HD], NT)
            gn[:, at] = acc

    for h in range(heads):
        keys_half(h)
        if h == 0:
            bulk_wait(gwz, nz - 1, ssem.at[GZ])
            bulk_wait(gwz_rcv, nz - 1, rsem.at[GZ])
            acc = gwz[z]
            for j in range(1, nz):
                acc += gwz_rcv[j]
            gw_ref[...] = acc

    @pl.loop(0, quarter // 32)
    def _(j):
        at = pl.ds(pl.multiple_of(j * 32, 32), 32)
        s = store[pl.ds(pl.multiple_of(x * quarter + j * 32, 32), 32), :].astype(F32)
        r = lax.rsqrt(jnp.mean(s * s, axis=-1, keepdims=True) + EPS)
        u = s * r
        g = gn[at, :] * gain_ref[...]
        gs_ref[at, :] = r * (g - u * jnp.mean(g * u, axis=-1, keepdims=True))

    bulk_wait(asked_v, nst - 1, ssem.at[REQ])
    bulk_wait(snd_b, nst - 1, ssem.at[V])
    bulk_wait(snd_a, nst - 1, ssem.at[DV])
    for h in range(heads):
        bulk_wait(dk_snd[h], nst - 1, ssem.at[DK + h])
        bulk_wait(own_k.at[h], nx - 1, ssem.at[XK + h])
    bulk_wait(wk_all, nx - 1, ssem.at[WK])
    bulk_wait(wv_all, nx - 1, ssem.at[WV])
    bulk_wait(own_v, nx - 1, ssem.at[XV])


def local(dims, queries, gate_pre, cotangent, store, store_gain, w_key, w_value, owners, slots):
    nz, ny, nc, nx = dims
    nst = nz * ny * nc
    blocks, per = owners.shape
    rows, width = store.shape
    tokens, cols = queries.shape
    heads = cols // HD
    npass = rows // PLEN
    count = blocks * per
    quarter = rows // nx
    piece = width // nst
    flat = owners.reshape(count)
    hits = flat[:, None] == jnp.arange(nst, dtype=jnp.int32)[None, :]
    req = jnp.max(jnp.where(hits, slots.reshape(count)[:, None], -1), axis=0)
    inv = jnp.max(jnp.where(hits, jnp.arange(count, dtype=jnp.int32)[:, None], 0), axis=0)
    req = jnp.broadcast_to(req[:, None, None], (nst, 1, 128))
    anywhere = pl.BlockSpec(memory_space=pl.ANY)
    vmem = pl.BlockSpec(memory_space=pltpu.VMEM)
    smem = pl.BlockSpec(memory_space=pltpu.SMEM)
    per_peer = pltpu.VMEM((nst, PLEN, cols), BF)
    per_head = pltpu.VMEM((nst, PLEN, HD), BF)
    return pl.pallas_call(
        functools.partial(kernel, (nz, ny, nc, nx, npass)),
        out_shape=(
            jax.ShapeDtypeStruct((tokens, cols), F32),
            jax.ShapeDtypeStruct((quarter, width), F32),
            jax.ShapeDtypeStruct((piece, cols), F32),
        ),
        in_specs=[anywhere] * 6 + [vmem, vmem, smem, smem],
        out_specs=(vmem, vmem, vmem),
        scratch_shapes=[
            pltpu.VMEM((rows, width), BF),
            pltpu.VMEM((rows, width), BF),
            pltpu.VMEM((nx, width, cols), BF),
            pltpu.VMEM((nx, width, cols), BF),
            pltpu.VMEM((tokens, cols), BF),
            pltpu.VMEM((tokens, cols), BF),
            pltpu.VMEM((tokens, cols), BF),
            pltpu.VMEM((npass, PLEN, cols), BF),
            per_peer,
            per_peer,
            per_peer,
            per_peer,
            per_peer,
            per_head,
            per_head,
            per_head,
            per_head,
            pltpu.VMEM((blocks * heads, per * PLEN, 128), F32),
            pltpu.VMEM((count, PLEN, cols), BF),
            per_peer,
            pltpu.VMEM((rows, cols), BF),
            pltpu.VMEM((heads, rows, HD), BF),
            pltpu.VMEM((nx, quarter, cols), BF),
            pltpu.VMEM((heads, nx, quarter, HD), BF),
            pltpu.VMEM((quarter, width), F32),
            pltpu.VMEM((nst, piece, cols), F32),
            pltpu.VMEM((nz * ny, piece, cols), F32),
            pltpu.VMEM((ny, nz, piece, cols), F32),
            pltpu.VMEM((ny, nz, piece, cols), F32),
            pltpu.VMEM((nz, piece, cols), F32),
            pltpu.VMEM((nz, piece, cols), F32),
            pltpu.VMEM((nst, 1, 128), jnp.int32),
            pltpu.VMEM((8, 128), jnp.int32),
            pltpu.SMEM((8, 128), jnp.int32),
            pltpu.SemaphoreType.DMA((11,)),
            pltpu.SemaphoreType.DMA((14,)),
            pltpu.SemaphoreType.DMA((14,)),
            pltpu.SemaphoreType.DMA((14,)),
        ],
        compiler_params=pltpu.CompilerParams(
            collective_id=0, has_side_effects=True, vmem_limit_bytes=67_043_328
        ),
    )(
        store,
        w_key,
        w_value,
        queries,
        gate_pre,
        cotangent,
        store_gain.reshape(1, width),
        req,
        flat,
        inv,
    )


def solution(mesh):
    nx = mesh.shape["tp"]
    nst = mesh.shape["st"]
    nz, ny, nc = nst // 8, 4, 2
    torus = Mesh(mesh.devices.reshape(nz, ny, nc, nx), ST_TP)
    return jax.shard_map(
        functools.partial(local, (nz, ny, nc, nx)),
        mesh=torus,
        in_specs=(
            P(ST, "tp"),
            P(ST, "tp"),
            P(ST, "tp"),
            P(ST, None),
            P(),
            P(None, "tp"),
            P(None, "tp"),
            P(ST, None),
            P(ST, None),
        ),
        out_specs=(P(ST, "tp"), P(ST_TP, None), P(ST, "tp")),
        check_vma=False,
    )
```

time: 499 us -> 236 us (0.47); the launches traced: 491 us -> 235 us
  waiting for transfers between devices: 230 us -> 0 us
  Pallas kernels: 0 us -> 225 us
  blocking collectives: 66.7 us -> 0 us
  local copies, waits for them, and re-layouts: 70.8 us -> 8.85 us
  starting transfers between devices: 49.1 us -> 0 us
  other arithmetic: 31.5 us -> 0.6 us
  matrix products: 27.9 us -> 0 us
  between operations: 14.9 us -> 0.64 us
    all_to_all x7 -> x0, waiting for transfers between devices: 230 us -> none  [the longest x1 85.7 us: local(): lax.all_to_all(outgoing_keys, ST, split_axis=0, concat_axis=0, tiled=True)]
    pallas_call x0 -> x1, Pallas kernels: none -> 225 us  [local(): pl.pallas_call(functools.partial(kernel, (nz, ny, nc, nx, npass)), out_sh...]
    all_to_all x2 -> x0, blocking collectives: 66.7 us -> none  [the longest x1 60.2 us: local(): lax.all_to_all(picked_values, ST, split_axis=0, concat_axis=0, tiled=True)]
    all_to_all x7 -> x0, starting transfers between devices: 48.9 us -> none  [the longest x1 9.6 us: sum_at_owner(): lax.all_to_all(blocks, axis, split_axis=0, concat_axis=0, tiled=True)]
    dot_general x13 -> x0, matrix products: 27.9 us -> none  [the longest x2 7.87 us: contract(): lax.dot_general(left, right, (((1,), (1,)), ((), ())), preferred_element_...]
    reshape x12 -> x0, local copies, waits for them, and re-layouts: 10.8 us -> none  [the longest x1 2.93 us: local(): grad_values = grad_values.reshape(slot_count, passage_len, local_width)]
    scatter x2 -> x0, local copies, waits for them, and re-layouts: 10.8 us -> none  [the longest x1 5.42 us: local(): outgoing_keys = empty_slots.at[position].set(grad_keys)]
    unnamed x46 -> x9, local copies, waits for them, and re-layouts: 17.6 us -> 7.94 us
  transfers between devices with their start and end apart: 8 -> 0, of which waited for: 5 -> 0; matrix products, arithmetic and copies ran while one was open for 19% -> 0% of each run, Pallas kernels for 0% -> 0%
where the time goes in v1:
time: 236 us; the launch traced here: 235 us
  Pallas kernels  225 us (95%)
  local copies, waits for them, and re-layouts  8.85 us (4%)
    pallas_call x1, Pallas kernels, local(): pl.pallas_call(functools.partial(kernel, (nz, ny, nc, nx, npass)), out_sh...  225 us
    unnamed x9, local copies, waits for them, and re-layouts  7.94 us

profile of v1, /device:TPU:1, one launch (start us, length us, event | category | flops | bytes accessed | tf_op | source)
XLA Modules:
  0.0 235.1 jit_solution(8609246369545073413)
XLA Ops:
  0.6 0.8 copy.16
  1.4 0.1 eq.15.pos_ref
  1.5 0.0 copy-start.1
  1.5 0.8 copy.17
  2.2 0.1 broadcast_in_dim.30
  2.3 0.0 copy-done.1
  2.3 0.6 select_reduce_fusion
  2.9 0.7 broadcast_in_dim.33.req_ref
  3.7 225.0 %shard_map.112 = (f32[1024,256]{1,0:T(8,128)}, f32[320,2048]{1,0:T(8,128)}, f32[32,256]{1,0:T(8,128)}) custom-call(bf16[1280,2048]{1,0:T(8,128)(2,1)} %store_hbm.1, bf16[2048,256]{1,0:T(8,128)(2,1)} %wk_hbm.1, bf16[2048,256]{1,0:T(8,128)(2,1)} %wv_hbm.1, bf16[1024,256]{1,0:T(8,128)(2,1)} %q_hbm.1, bf16[1024,256]{1,0:T(8,128)(2,1)} %gate_hbm.1, ...), custom_call_target="tpu_custom_call" | custom-call | tf_op jit(solution)/shard_map/pallas_call | solution.py:489
  228.7 2.3 copy.21
  230.9 0.0 copy-start
  230.9 3.5 %copy.22 = f32[320,2048]{1,0:T(8,128)} copy(f32[320,2048]{1,0:T(8,128)} %get-tuple-element.9) | data formatting | bytes 5242880
  234.5 0.0 copy-done
  234.5 0.6 copy.23
Async XLA Ops:
  1.5 0.8 copy-start.1
  230.9 3.5 %copy-start = (f32[32,256]{1,0:T(8,128)S(1)}, f32[32,256]{1,0:T(8,128)}, u32[]{:S(2)}) copy-start(f32[32,256]{1,0:T(8,128)} %get-tuple-element.10) | copy-start | bytes 98308

commit v2 on v1

--- a/solution.py
+++ b/solution.py
@@ -35,9 +35,8 @@
     gate_hbm,
     cot_hbm,
     gain_ref,
-    req_ref,
-    pos_ref,
-    inv_ref,
+    owners_ref,
+    slots_ref,
     dq_ref,
     gs_ref,
     gw_ref,
@@ -56,15 +55,21 @@
     dv_rcv,
     dk_snd_0,
     dk_snd_1,
+    dk_snd_2,
     dk_rcv_0,
     dk_rcv_1,
+    dk_rcv_2,
     wts,
     slot_a,
     run,
     pas_v,
-    pas_k,
+    pas_k_0,
+    pas_k_1,
+    pas_k_2,
     own_v,
-    own_k,
+    own_k_0,
+    own_k_1,
+    own_k_2,
     gn,
     gw_full,
     gwc_rcv,
@@ -72,6 +77,7 @@
     gwy_rcv,
     gwz,
     gwz_rcv,
+    req_ref,
     asked_v,
     meta_v,
     meta_s,
@@ -82,19 +88,20 @@
 ):
     nz, ny, nc, nx, npass = cfg
     nst = nz * ny * nc
-    dk_snd = (dk_snd_0, dk_snd_1)
-    dk_rcv = (dk_rcv_0, dk_rcv_1)
+    dk_snd = (dk_snd_0, dk_snd_1, dk_snd_2)
+    dk_rcv = (dk_rcv_0, dk_rcv_1, dk_rcv_2)
+    pas_k = (pas_k_0, pas_k_1, pas_k_2)
+    own_k = (own_k_0, own_k_1, own_k_2)
     rows, width = store.shape
     heads = wk_all.shape[2] // HD
-    blocks = q.shape[0] // 128
-    per = pos_ref.shape[0] // blocks
+    blocks, per = owners_ref.shape
     quarter = rows // nx
     z = lax.axis_index("st_0")
     y = lax.axis_index("st_1")
     c = lax.axis_index("st_2")
     x = lax.axis_index("tp")
     me = (z * ny + y) * nc + c
-    WV, REQ, K, V, DV, DK, WK, XV, XK, GC, GY, GZ = 0, 1, 2, 3, 4, 5, 7, 8, 9, 11, 12, 13
+    REQ, K, V, DV, WK, WV, XV, GC, GY, GZ, DK, XK = 0, 1, 2, 3, 4, 5, 6, 7, 8, 9, 10, 13
 
     def st_peer(i):
         pz = lax.rem(z + i // (ny * nc), nz)
@@ -135,7 +142,6 @@
     load_q.start()
     load_g.start()
     load_c.start()
-    pl.semaphore_wait(barrier, nst + nx - 2)
 
     def send_st(src, dst, k):
         @pl.loop(1, nst)
@@ -158,11 +164,23 @@
         part = buf.at[pl.ds(0, n)]
         pltpu.make_async_copy(part, part, sem).wait()
 
-    own_req = send_st(req_ref, asked_v, REQ)
+    lane = lax.broadcasted_iota(jnp.int32, (nst, 128), 1)
+    row = lax.broadcasted_iota(jnp.int32, (nst, 128), 0)
+    req = jnp.full((nst, 128), -1, jnp.int32)
+    place_row = jnp.zeros((1, 128), jnp.int32)
+    for b in range(blocks):
+        for j in range(per):
+            req = jnp.where(row == owners_ref[b, j], slots_ref[b, j], req)
+            place_row = jnp.where(lane[0:1] == owners_ref[b, j], b * per + j, place_row)
+    req_ref[...] = req.reshape(nst, 1, 128)
+    meta_v[5:6, :] = place_row
 
     load_k.wait()
     for i in range(5):
         loads[i].wait()
+        if i == 2:
+            pl.semaphore_wait(barrier, nst + nx - 2)
+            own_req = send_st(req_ref, asked_v, REQ)
 
         @pl.loop(0, chunk // 64)
         def _(j):
@@ -179,8 +197,6 @@
     own_req.wait()
     bulk_wait(asked_v, nst - 1, rsem.at[REQ])
     asked = asked_v[...].reshape(nst, 128)
-    lane = lax.broadcasted_iota(jnp.int32, (nst, 128), 1)
-    row = lax.broadcasted_iota(jnp.int32, (nst, 128), 0)
     slot_col = jnp.where(asked < 0, npass, asked)
     key_col = slot_col * nst + row
     diag = lane == row
@@ -248,7 +264,7 @@
     scale = HD ** (-0.5)
 
     def passages(ref, b, h):
-        parts = [ref[pos_ref[b * per + j], :, h * HD : (h + 1) * HD] for j in range(per)]
+        parts = [ref[owners_ref[b, j], :, h * HD : (h + 1) * HD] for j in range(per)]
         return jnp.concatenate(parts, axis=0)
 
     own_k_copy.wait()
@@ -272,19 +288,18 @@
 
     @pl.loop(0, nst)
     def _(t):
-        snd_a[t] = slot_a[inv_ref[t]]
+        snd_a[t] = slot_a[meta_s[5, t]]
 
     own_dv_copy = send_st(snd_a, dv_rcv, DV)
 
     own_v_copy.wait()
     bulk_wait(v_rcv, nst - 1, rsem.at[V])
 
-    for h in range(heads):
-        cols = slice(h * HD, (h + 1) * HD)
-
-        @pl.loop(0, blocks)
-        def _(b):
-            at = pl.ds(pl.multiple_of(b * 128, 128), 128)
+    @pl.loop(0, blocks)
+    def _(b):
+        at = pl.ds(pl.multiple_of(b * 128, 128), 128)
+        for h in range(heads):
+            cols = slice(h * HD, (h + 1) * HD)
             kh = passages(k_rcv, b, h)
             vh = passages(v_rcv, b, h)
             gwt = dot(vh, gin[at, cols], NT)
@@ -294,35 +309,47 @@
             dk = (dot(gsc, q[at, cols]) * scale).astype(BF)
             for j in range(per):
                 slot_a[b * per + j, :, cols] = dk[j * PLEN : (j + 1) * PLEN]
-            dq_ref[at, cols] = dot(gsc, kh, TN) * scale
+            dq_ref[at, cols] = (dot(gsc, kh, TN) * scale).astype(BF)
+
+    half = PLEN // 2
+    pieces = (
+        (0, slice(0, heads * HD)),
+        (1, slice(0, HD)),
+        (1, slice(HD, heads * HD)),
+    )
+
+    def send_piece(k):
+        part, cols = pieces[k]
 
         @pl.loop(0, nst)
         def _(t):
-            dk_snd[h][t] = slot_a[inv_ref[t], :, cols]
-
-        send_st(dk_snd[h], dk_rcv[h], DK + h)
-
-    def owner_sum(rcv, cols, out):
+            dk_snd[k][t] = slot_a[meta_s[5, t], part * half : (part + 1) * half, cols]
+
+        send_st(dk_snd[k], dk_rcv[k], DK + k)
+
+    send_piece(0)
+
+    def owner_sum(rcv, run, out):
         def step(i, acc):
             acc = acc * meta_s[2, i].astype(F32) + rcv[meta_s[1, i]].astype(F32)
-            run[i, :, cols] = acc.astype(BF)
+            run[i] = acc.astype(BF)
             return acc
 
-        wide = cols.stop - cols.start
-        lax.fori_loop(0, nst, step, jnp.zeros((PLEN, wide), F32))
+        lax.fori_loop(0, nst, step, jnp.zeros(rcv.shape[1:], F32))
 
         @pl.loop(0, npass)
         def _(p):
-            got = run[meta_s[3, p], :, cols].astype(F32)
-            some = meta_s[4, p].astype(F32)
-            out[pl.ds(pl.multiple_of(p * PLEN, PLEN), PLEN), :] = (got * some).astype(BF)
+            got = run[meta_s[3, p]].astype(F32)
+            out[p] = (got * meta_s[4, p].astype(F32)).astype(BF)
+
+    few = npass // nx
 
     def send_x(src, dst, k):
         @pl.loop(1, nx)
         def _(i):
             device, px = x_peer(i)
             pltpu.make_async_remote_copy(
-                src_ref=src.at[pl.ds(pl.multiple_of(px * quarter, 64), quarter)],
+                src_ref=src.at[pl.ds(px * few, few)],
                 dst_ref=dst.at[x],
                 send_sem=ssem.at[k],
                 recv_sem=rsem.at[k],
@@ -330,19 +357,17 @@
                 device_id_type=MESH,
             ).start()
 
-        own = pltpu.make_async_copy(
-            src.at[pl.ds(pl.multiple_of(x * quarter, 64), quarter)], dst.at[x], self_sem.at[k]
-        )
+        own = pltpu.make_async_copy(src.at[pl.ds(x * few, few)], dst.at[x], self_sem.at[k])
         own.start()
         return own
 
     own_dv_copy.wait()
     bulk_wait(dv_rcv, nst - 1, rsem.at[DV])
-    owner_sum(dv_rcv, slice(0, heads * HD), pas_v)
+    owner_sum(dv_rcv, run, pas_v)
     own_xv = send_x(pas_v, own_v, XV)
 
     tile = 256
-    pv_t = pas_v[...].T
+    pv_t = pas_v[...].reshape(rows, heads * HD).T
 
     @pl.loop(0, width // tile)
     def _(j):
@@ -364,25 +389,12 @@
     )
     to_core.start()
 
-    bulk_wait(wk_all, nx - 1, rsem.at[WK])
-    bulk_wait(wv_all, nx - 1, rsem.at[WV])
-    own_xv.wait()
-    bulk_wait(own_v, nx - 1, rsem.at[XV])
-
-    @pl.loop(0, width // tile)
-    def _(j):
-        at = pl.ds(pl.multiple_of(j * tile, tile), tile)
-        acc = dot(own_v[0], wv_all[0, at, :], NT)
-        for s in range(1, nx):
-            acc += dot(own_v[s], wv_all[s, at, :], NT)
-        gn[:, at] = acc
-
     to_core.wait()
 
     @pl.loop(0, nz * ny)
     def _(i):
         zi, yi = i // ny, lax.rem(i, ny)
-        gwy[yi, zi] = gw_full[i * nc + c] + gwc_rcv[i]
+        gwy[yi, zi] = (gw_full[i * nc + c] + gwc_rcv[i]).astype(BF)
 
     @pl.loop(1, ny)
     def _(i):
@@ -396,15 +408,65 @@
             device_id_type=MESH,
         ).start()
 
+    send_piece(1)
+    send_piece(2)
+
+    bulk_wait(wk_all, nx - 1, rsem.at[WK])
+    bulk_wait(wv_all, nx - 1, rsem.at[WV])
+    own_xv.wait()
+    bulk_wait(own_v, nx - 1, rsem.at[XV])
+
+    @pl.loop(0, width // tile)
+    def _(j):
+        at = pl.ds(pl.multiple_of(j * tile, tile), tile)
+        acc = dot(own_v[0].reshape(quarter, heads * HD), wv_all[0, at, :], NT)
+        for s in range(1, nx):
+            acc += dot(own_v[s].reshape(quarter, heads * HD), wv_all[s, at, :], NT)
+        acc = acc.reshape(few, 2, half, tile)
+        gn[0, :, at] = acc[:, 0].reshape(few * half, tile)
+        gn[1, :, at] = acc[:, 1].reshape(few * half, tile)
+
+    def keys_piece(k):
+        part, cols = pieces[k]
+        own = pltpu.make_async_copy(dk_snd[k].at[me], dk_rcv[k].at[me], self_sem.at[DK + k])
+        own.wait()
+        bulk_wait(dk_rcv[k], nst - 1, rsem.at[DK + k])
+        bulk_wait(dk_snd[k], nst - 1, ssem.at[DK + k])
+        owner_sum(dk_rcv[k], dk_snd[k], pas_k[k])
+        own_x = send_x(pas_k[k], own_k[k], XK + k)
+        own_x.wait()
+        bulk_wait(own_k[k], nx - 1, rsem.at[XK + k])
+
+        @pl.loop(0, width // tile)
+        def _(j):
+            at = pl.ds(pl.multiple_of(j * tile, tile), tile)
+            acc = gn[part, :, at]
+            for s in range(nx):
+                mine = own_k[k][s].reshape(few * half, cols.stop - cols.start)
+                acc += dot(mine, wk_all[s, at, cols], NT)
+            gn[part, :, at] = acc
+
+    def finish(part):
+        @pl.loop(0, few)
+        def _(j):
+            at = pl.ds(pl.multiple_of(j * PLEN + part * half, half), half)
+            first = x * quarter + j * PLEN + part * half
+            s = store[pl.ds(pl.multiple_of(first, half), half), :].astype(F32)
+            r = lax.rsqrt(jnp.mean(s * s, axis=-1, keepdims=True) + EPS)
+            u = s * r
+            g = gn[part, pl.ds(pl.multiple_of(j * half, half), half), :] * gain_ref[...]
+            gs_ref[at, :] = (r * (g - u * jnp.mean(g * u, axis=-1, keepdims=True))).astype(BF)
+
+    keys_piece(0)
     bulk_wait(gwy, ny - 1, ssem.at[GY])
     bulk_wait(gwy_rcv, ny - 1, rsem.at[GY])
 
     @pl.loop(0, nz)
     def _(i):
-        acc = gwy[y, i]
+        acc = gwy[y, i].astype(F32)
         for j in range(1, ny):
-            acc += gwy_rcv[j, i]
-        gwz[i] = acc
+            acc += gwy_rcv[j, i].astype(F32)
+        gwz[i] = acc.astype(BF)
 
     @pl.loop(1, nz)
     def _(i):
@@ -418,48 +480,22 @@
             device_id_type=MESH,
         ).start()
 
-    def keys_half(h):
-        own = pltpu.make_async_copy(dk_snd[h].at[me], dk_rcv[h].at[me], self_sem.at[DK + h])
-        own.wait()
-        bulk_wait(dk_rcv[h], nst - 1, rsem.at[DK + h])
-        owner_sum(dk_rcv[h], slice(0, HD), pas_k.at[h])
-        own_x = send_x(pas_k.at[h], own_k.at[h], XK + h)
-        own_x.wait()
-        bulk_wait(own_k.at[h], nx - 1, rsem.at[XK + h])
-
-        @pl.loop(0, width // tile)
-        def _(j):
-            at = pl.ds(pl.multiple_of(j * tile, tile), tile)
-            acc = gn[:, at]
-            for s in range(nx):
-                acc += dot(own_k[h, s], wk_all[s, at, h * HD : (h + 1) * HD], NT)
-            gn[:, at] = acc
-
-    for h in range(heads):
-        keys_half(h)
-        if h == 0:
-            bulk_wait(gwz, nz - 1, ssem.at[GZ])
-            bulk_wait(gwz_rcv, nz - 1, rsem.at[GZ])
-            acc = gwz[z]
-            for j in range(1, nz):
-                acc += gwz_rcv[j]
-            gw_ref[...] = acc
-
-    @pl.loop(0, quarter // 32)
-    def _(j):
-        at = pl.ds(pl.multiple_of(j * 32, 32), 32)
-        s = store[pl.ds(pl.multiple_of(x * quarter + j * 32, 32), 32), :].astype(F32)
-        r = lax.rsqrt(jnp.mean(s * s, axis=-1, keepdims=True) + EPS)
-        u = s * r
-        g = gn[at, :] * gain_ref[...]
-        gs_ref[at, :] = r * (g - u * jnp.mean(g * u, axis=-1, keepdims=True))
+    finish(0)
+    keys_piece(1)
+    keys_piece(2)
+    finish(1)
+    bulk_wait(gwz, nz - 1, ssem.at[GZ])
+    bulk_wait(gwz_rcv, nz - 1, rsem.at[GZ])
+    acc = gwz[z].astype(F32)
+    for j in range(1, nz):
+        acc += gwz_rcv[j].astype(F32)
+    gw_ref[...] = acc
 
     bulk_wait(asked_v, nst - 1, ssem.at[REQ])
     bulk_wait(snd_b, nst - 1, ssem.at[V])
     bulk_wait(snd_a, nst - 1, ssem.at[DV])
-    for h in range(heads):
-        bulk_wait(dk_snd[h], nst - 1, ssem.at[DK + h])
-        bulk_wait(own_k.at[h], nx - 1, ssem.at[XK + h])
+    for k in range(3):
+        bulk_wait(own_k[k], nx - 1, ssem.at[XK + k])
     bulk_wait(wk_all, nx - 1, ssem.at[WK])
     bulk_wait(wv_all, nx - 1, ssem.at[WV])
     bulk_wait(own_v, nx - 1, ssem.at[XV])
@@ -476,24 +512,22 @@
     count = blocks * per
     quarter = rows // nx
     piece = width // nst
-    flat = owners.reshape(count)
-    hits = flat[:, None] == jnp.arange(nst, dtype=jnp.int32)[None, :]
-    req = jnp.max(jnp.where(hits, slots.reshape(count)[:, None], -1), axis=0)
-    inv = jnp.max(jnp.where(hits, jnp.arange(count, dtype=jnp.int32)[:, None], 0), axis=0)
-    req = jnp.broadcast_to(req[:, None, None], (nst, 1, 128))
     anywhere = pl.BlockSpec(memory_space=pl.ANY)
     vmem = pl.BlockSpec(memory_space=pltpu.VMEM)
     smem = pl.BlockSpec(memory_space=pltpu.SMEM)
     per_peer = pltpu.VMEM((nst, PLEN, cols), BF)
-    per_head = pltpu.VMEM((nst, PLEN, HD), BF)
-    return pl.pallas_call(
+    half = PLEN // 2
+    few = npass // nx
+    wide = pltpu.VMEM((nst, half, cols), BF)
+    narrow = pltpu.VMEM((nst, half, HD), BF)
+    dq, gs, gw = pl.pallas_call(
         functools.partial(kernel, (nz, ny, nc, nx, npass)),
         out_shape=(
-            jax.ShapeDtypeStruct((tokens, cols), F32),
-            jax.ShapeDtypeStruct((quarter, width), F32),
+            jax.ShapeDtypeStruct((tokens, cols), BF),
+            jax.ShapeDtypeStruct((quarter, width), BF),
             jax.ShapeDtypeStruct((piece, cols), F32),
         ),
-        in_specs=[anywhere] * 6 + [vmem, vmem, smem, smem],
+        in_specs=[anywhere] * 6 + [vmem, smem, smem],
         out_specs=(vmem, vmem, vmem),
         scratch_shapes=[
             pltpu.VMEM((rows, width), BF),
@@ -509,31 +543,38 @@
             per_peer,
             per_peer,
             per_peer,
-            per_head,
-            per_head,
-            per_head,
-            per_head,
+            wide,
+            narrow,
+            narrow,
+            wide,
+            narrow,
+            narrow,
             pltpu.VMEM((blocks * heads, per * PLEN, 128), F32),
             pltpu.VMEM((count, PLEN, cols), BF),
             per_peer,
-            pltpu.VMEM((rows, cols), BF),
-            pltpu.VMEM((heads, rows, HD), BF),
-            pltpu.VMEM((nx, quarter, cols), BF),
-            pltpu.VMEM((heads, nx, quarter, HD), BF),
-            pltpu.VMEM((quarter, width), F32),
+            pltpu.VMEM((npass, PLEN, cols), BF),
+            pltpu.VMEM((npass, half, cols), BF),
+            pltpu.VMEM((npass, half, HD), BF),
+            pltpu.VMEM((npass, half, HD), BF),
+            pltpu.VMEM((nx, few, PLEN, cols), BF),
+            pltpu.VMEM((nx, few, half, cols), BF),
+            pltpu.VMEM((nx, few, half, HD), BF),
+            pltpu.VMEM((nx, few, half, HD), BF),
+            pltpu.VMEM((2, few * half, width), F32),
             pltpu.VMEM((nst, piece, cols), F32),
             pltpu.VMEM((nz * ny, piece, cols), F32),
-            pltpu.VMEM((ny, nz, piece, cols), F32),
-            pltpu.VMEM((ny, nz, piece, cols), F32),
-            pltpu.VMEM((nz, piece, cols), F32),
-            pltpu.VMEM((nz, piece, cols), F32),
+            pltpu.VMEM((ny, nz, piece, cols), BF),
+            pltpu.VMEM((ny, nz, piece, cols), BF),
+            pltpu.VMEM((nz, piece, cols), BF),
+            pltpu.VMEM((nz, piece, cols), BF),
+            pltpu.VMEM((nst, 1, 128), jnp.int32),
             pltpu.VMEM((nst, 1, 128), jnp.int32),
             pltpu.VMEM((8, 128), jnp.int32),
             pltpu.SMEM((8, 128), jnp.int32),
             pltpu.SemaphoreType.DMA((11,)),
-            pltpu.SemaphoreType.DMA((14,)),
-            pltpu.SemaphoreType.DMA((14,)),
-            pltpu.SemaphoreType.DMA((14,)),
+            pltpu.SemaphoreType.DMA((16,)),
+            pltpu.SemaphoreType.DMA((16,)),
+            pltpu.SemaphoreType.DMA((16,)),
         ],
         compiler_params=pltpu.CompilerParams(
             collective_id=0, has_side_effects=True, vmem_limit_bytes=67_043_328
@@ -546,10 +587,10 @@
         gate_pre,
         cotangent,
         store_gain.reshape(1, width),
-        req,
-        flat,
-        inv,
+        owners,
+        slots,
     )
+    return dq.astype(F32), gs.astype(F32), gw
 
 
 def solution(mesh):

time: 236 us -> 225 us (0.953)
  Pallas kernels: 225 us -> 216 us
  local copies, waits for them, and re-layouts: 8.85 us -> 3.32 us
  other arithmetic: 0.6 us -> 4.22 us
    pallas_call x1, Pallas kernels: 225 us -> 216 us  [local(): pl.pallas_call(functools.partial(kernel, (nz, ny, nc, nx, npass)), out_sh...]
    unnamed x9 -> x7, local copies, waits for them, and re-layouts: 7.94 us -> 3.32 us
    convert_element_type x0 -> x2, other arithmetic: none -> 4.22 us  [local(): return (dq.astype(F32), gs.astype(F32), gw)]
where the time goes in v2:
time: 225 us
  Pallas kernels  216 us (96%)
  other arithmetic  4.22 us (2%)
  local copies, waits for them, and re-layouts  3.32 us (1%)
    pallas_call x1, Pallas kernels, local(): pl.pallas_call(functools.partial(kernel, (nz, ny, nc, nx, npass)), out_sh...  216 us

profile of v2, /device:TPU:1, one launch (start us, length us, event | category | flops | bytes accessed | tf_op | source)
XLA Modules:
  0.0 224.7 jit_solution(9451093713900630844)
XLA Ops:
  0.6 1.3 copy.12.owners_ref
  2.0 1.3 copy.13.slots_ref
  3.3 216.5 %shard_map.112 = (bf16[1024,256]{1,0:T(8,128)(2,1)}, bf16[320,2048]{1,0:T(8,128)(2,1)}, f32[32,256]{1,0:T(8,128)}) custom-call(bf16[1280,2048]{1,0:T(8,128)(2,1)} %store_hbm.1, bf16[2048,256]{1,0:T(8,128)(2,1)} %wk_hbm.1, bf16[2048,256]{1,0:T(8,128)(2,1)} %wv_hbm.1, bf16[1024,256]{1,0:T(8,128)(2,1)} %q_hbm.1, bf16[1024,256]{1,0:T(8,128)(2,1)} %gate_hbm.1, ...), custom_call_target="tpu_custom_call" | custom-call | tf_op jit(solution)/shard_map/pallas_call | solution.py:523
  219.8 0.0 copy-start
  219.8 0.0 copy-start.1
  219.8 3.2 %convert_element_type.7 = f32[320,2048]{1,0:T(8,128)} convert(bf16[320,2048]{1,0:T(8,128)(2,1)} %get-tuple-element.7) | non-fusion elementwise | flops 655360 | bytes 3932160 | tf_op jit(solution)/shard_map/convert_element_type | solution.py:593
  223.0 0.0 copy-done
  223.0 1.0 convert_element_type.6
  224.0 0.0 copy-done.1
  224.0 0.6 copy.15
Async XLA Ops:
  219.8 3.2 %copy-start = (bf16[1024,256]{1,0:T(8,128)(2,1)S(1)}, bf16[1024,256]{1,0:T(8,128)(2,1)}, u32[]{:S(2)}) copy-start(bf16[1024,256]{1,0:T(8,128)(2,1)} %get-tuple-element.6) | copy-start | bytes 1572868
  219.8 4.2 %copy-start.1 = (f32[32,256]{1,0:T(8,128)S(1)}, f32[32,256]{1,0:T(8,128)}, u32[]{:S(2)}) copy-start(f32[32,256]{1,0:T(8,128)} %get-tuple-element.14) | copy-start | bytes 98308

commit v3 on v2

--- a/solution.py
+++ b/solution.py
@@ -34,9 +34,9 @@
     q_hbm,
     gate_hbm,
     cot_hbm,
-    gain_ref,
-    owners_ref,
-    slots_ref,
+    gain_hbm,
+    owners_hbm,
+    slots_hbm,
     dq_ref,
     gs_ref,
     gw_ref,
@@ -81,6 +81,9 @@
     asked_v,
     meta_v,
     meta_s,
+    gain_ref,
+    owners_ref,
+    slots_ref,
     load_sem,
     self_sem,
     ssem,
@@ -94,7 +97,7 @@
     own_k = (own_k_0, own_k_1, own_k_2)
     rows, width = store.shape
     heads = wk_all.shape[2] // HD
-    blocks, per = owners_ref.shape
+    per, blocks = owners_ref.shape
     quarter = rows // nx
     z = lax.axis_index("st_0")
     y = lax.axis_index("st_1")
@@ -103,11 +106,19 @@
     me = (z * ny + y) * nc + c
     REQ, K, V, DV, WK, WV, XV, GC, GY, GZ, DK, XK = 0, 1, 2, 3, 4, 5, 6, 7, 8, 9, 10, 13
 
-    def st_peer(i):
-        pz = lax.rem(z + i // (ny * nc), nz)
-        py = lax.rem(y + lax.rem(i // nc, ny), ny)
-        pc = lax.rem(c + lax.rem(i, nc), nc)
-        return (pz, py, pc, x), (pz * ny + py) * nc + pc
+    def each_st(act):
+        others = [
+            (lax.rem(y + dy, ny), lax.rem(c + dc, nc)) for dy in range(ny) for dc in range(nc)
+        ]
+
+        @pl.loop(1, nz)
+        def _(dz):
+            pz = lax.rem(z + dz, nz)
+            for py, pc in others:
+                act((pz, py, pc, x), (pz * ny + py) * nc + pc)
+
+        for py, pc in others[1:]:
+            act((z, py, pc, x), (z * ny + py) * nc + pc)
 
     def x_peer(i):
         px = lax.rem(x + i, nx)
@@ -115,9 +126,11 @@
 
     barrier = pltpu.get_barrier_semaphore()
 
-    @pl.loop(1, nst)
-    def _(i):
-        pl.semaphore_signal(barrier, inc=1, device_id=st_peer(i)[0], device_id_type=MESH)
+    each_st(
+        lambda device, t: pl.semaphore_signal(
+            barrier, inc=1, device_id=device, device_id_type=MESH
+        )
+    )
 
     @pl.loop(1, nx)
     def _(i):
@@ -135,6 +148,14 @@
     load_q = pltpu.make_async_copy(q_hbm, q, load_sem.at[7])
     load_g = pltpu.make_async_copy(gate_hbm, gate, load_sem.at[8])
     load_c = pltpu.make_async_copy(cot_hbm, gin, load_sem.at[9])
+    small = [
+        pltpu.make_async_copy(src, dst, load_sem.at[11 + i])
+        for i, (src, dst) in enumerate(
+            ((owners_hbm, owners_ref), (slots_hbm, slots_ref), (gain_hbm, gain_ref))
+        )
+    ]
+    for cp in small:
+        cp.start()
     load_k.start()
     for cp in loads:
         cp.start()
@@ -144,9 +165,7 @@
     load_c.start()
 
     def send_st(src, dst, k):
-        @pl.loop(1, nst)
-        def _(i):
-            device, t = st_peer(i)
+        def start(device, t):
             pltpu.make_async_remote_copy(
                 src_ref=src.at[t],
                 dst_ref=dst.at[me],
@@ -156,6 +175,7 @@
                 device_id_type=MESH,
             ).start()
 
+        each_st(start)
         own = pltpu.make_async_copy(src.at[me], dst.at[me], self_sem.at[k])
         own.start()
         return own
@@ -168,10 +188,12 @@
     row = lax.broadcasted_iota(jnp.int32, (nst, 128), 0)
     req = jnp.full((nst, 128), -1, jnp.int32)
     place_row = jnp.zeros((1, 128), jnp.int32)
+    for cp in small:
+        cp.wait()
     for b in range(blocks):
         for j in range(per):
-            req = jnp.where(row == owners_ref[b, j], slots_ref[b, j], req)
-            place_row = jnp.where(lane[0:1] == owners_ref[b, j], b * per + j, place_row)
+            req = jnp.where(row == owners_ref[j, b], slots_ref[j, b], req)
+            place_row = jnp.where(lane[0:1] == owners_ref[j, b], b * per + j, place_row)
     req_ref[...] = req.reshape(nst, 1, 128)
     meta_v[5:6, :] = place_row
 
@@ -264,7 +286,7 @@
     scale = HD ** (-0.5)
 
     def passages(ref, b, h):
-        parts = [ref[owners_ref[b, j], :, h * HD : (h + 1) * HD] for j in range(per)]
+        parts = [ref[owners_ref[j, b], :, h * HD : (h + 1) * HD] for j in range(per)]
         return jnp.concatenate(parts, axis=0)
 
     own_k_copy.wait()
@@ -514,7 +536,6 @@
     piece = width // nst
     anywhere = pl.BlockSpec(memory_space=pl.ANY)
     vmem = pl.BlockSpec(memory_space=pltpu.VMEM)
-    smem = pl.BlockSpec(memory_space=pltpu.SMEM)
     per_peer = pltpu.VMEM((nst, PLEN, cols), BF)
     half = PLEN // 2
     few = npass // nx
@@ -527,7 +548,7 @@
             jax.ShapeDtypeStruct((quarter, width), BF),
             jax.ShapeDtypeStruct((piece, cols), F32),
         ),
-        in_specs=[anywhere] * 6 + [vmem, smem, smem],
+        in_specs=[anywhere] * 9,
         out_specs=(vmem, vmem, vmem),
         scratch_shapes=[
             pltpu.VMEM((rows, width), BF),
@@ -571,7 +592,10 @@
             pltpu.VMEM((nst, 1, 128), jnp.int32),
             pltpu.VMEM((8, 128), jnp.int32),
             pltpu.SMEM((8, 128), jnp.int32),
-            pltpu.SemaphoreType.DMA((11,)),
+            pltpu.VMEM((1, width), F32),
+            pltpu.SMEM((per, blocks), jnp.int32),
+            pltpu.SMEM((per, blocks), jnp.int32),
+            pltpu.SemaphoreType.DMA((14,)),
             pltpu.SemaphoreType.DMA((16,)),
             pltpu.SemaphoreType.DMA((16,)),
             pltpu.SemaphoreType.DMA((16,)),
@@ -587,8 +611,8 @@
         gate_pre,
         cotangent,
         store_gain.reshape(1, width),
-        owners,
-        slots,
+        owners.T,
+        slots.T,
     )
     return dq.astype(F32), gs.astype(F32), gw
 

time: 225 us -> 220 us (0.978)
  local copies, waits for them, and re-layouts: 3.32 us -> 0.62 us
    unnamed x7 -> x5, local copies, waits for them, and re-layouts: 3.32 us -> 0.62 us
    pallas_call x1, Pallas kernels: 216 us -> 214 us  [local(): pl.pallas_call(functools.partial(kernel, (nz, ny, nc, nx, npass)), out_sh...]
where the time goes in v3:
time: 220 us
  Pallas kernels  214 us (97%)
  other arithmetic  4.22 us (2%)
    pallas_call x1, Pallas kernels, local(): pl.pallas_call(functools.partial(kernel, (nz, ny, nc, nx, npass)), out_sh...  214 us

profile of v3, /device:TPU:1, one launch (start us, length us, event | category | flops | bytes accessed | tf_op | source)
XLA Modules:
  0.0 219.6 jit_solution(11153359585745201073)
XLA Ops:
  0.6 214.1 %shard_map.112 = (bf16[1024,256]{1,0:T(8,128)(2,1)}, bf16[320,2048]{1,0:T(8,128)(2,1)}, f32[32,256]{1,0:T(8,128)}) custom-call(bf16[1280,2048]{1,0:T(8,128)(2,1)} %store_hbm.1, bf16[2048,256]{1,0:T(8,128)(2,1)} %wk_hbm.1, bf16[2048,256]{1,0:T(8,128)(2,1)} %wv_hbm.1, bf16[1024,256]{1,0:T(8,128)(2,1)} %q_hbm.1, bf16[1024,256]{1,0:T(8,128)(2,1)} %gate_hbm.1, ...), custom_call_target="tpu_custom_call" | custom-call | tf_op jit(solution)/shard_map/pallas_call | solution.py:544
  214.8 0.0 copy-start
  214.8 0.0 copy-start.1
  214.8 3.2 %convert_element_type.7 = f32[320,2048]{1,0:T(8,128)} convert(bf16[320,2048]{1,0:T(8,128)(2,1)} %get-tuple-element.7) | non-fusion elementwise | flops 655360 | bytes 3932160 | tf_op jit(solution)/shard_map/convert_element_type | solution.py:617
  218.0 0.0 copy-done
  218.0 1.0 convert_element_type.6
  219.0 0.0 copy-done.1
  219.0 0.6 copy.13
Async XLA Ops:
  214.8 3.2 %copy-start = (bf16[1024,256]{1,0:T(8,128)(2,1)S(1)}, bf16[1024,256]{1,0:T(8,128)(2,1)}, u32[]{:S(2)}) copy-start(bf16[1024,256]{1,0:T(8,128)(2,1)} %get-tuple-element.6) | copy-start | bytes 1572868
  214.8 4.2 %copy-start.1 = (f32[32,256]{1,0:T(8,128)S(1)}, f32[32,256]{1,0:T(8,128)}, u32[]{:S(2)}) copy-start(f32[32,256]{1,0:T(8,128)} %get-tuple-element.14) | copy-start | bytes 98308

commit v4 on v3

--- a/solution.py
+++ b/solution.py
@@ -106,19 +106,26 @@
     me = (z * ny + y) * nc + c
     REQ, K, V, DV, WK, WV, XV, GC, GY, GZ, DK, XK = 0, 1, 2, 3, 4, 5, 6, 7, 8, 9, 10, 13
 
+    far_z = sorted(range(nz), key=lambda d: (-min(d, nz - d), d))
+    far_y = sorted(range(ny), key=lambda d: (-min(d, ny - d), d))
+
     def each_st(act):
-        others = [
-            (lax.rem(y + dy, ny), lax.rem(c + dc, nc)) for dy in range(ny) for dc in range(nc)
-        ]
-
-        @pl.loop(1, nz)
-        def _(dz):
-            pz = lax.rem(z + dz, nz)
-            for py, pc in others:
+        def column(dy, dc, planes):
+            py = lax.rem(y + dy, ny)
+            pc = lax.rem(c + dc, nc)
+            for dz in planes:
+                pz = lax.rem(z + dz, nz)
                 act((pz, py, pc, x), (pz * ny + py) * nc + pc)
 
-        for py, pc in others[1:]:
-            act((z, py, pc, x), (z * ny + py) * nc + pc)
+        for dy in far_y[:-1]:
+
+            @pl.loop(0, nc)
+            def _(dc):
+                column(dy, dc, far_z)
+
+        column(0, 0, far_z[:-1])
+        for dc in range(1, nc):
+            column(0, dc, far_z)
 
     def x_peer(i):
         px = lax.rem(x + i, nx)

time: 220 us -> 218 us (level)
  no operation moved by 1% of the time
where the time goes in v4:
time: 218 us
  Pallas kernels  212 us (97%)
  other arithmetic  4.22 us (2%)
    pallas_call x1, Pallas kernels, local(): pl.pallas_call(functools.partial(kernel, (nz, ny, nc, nx, npass)), out_sh...  212 us

profile of v4, /device:TPU:1, one launch (start us, length us, event | category | flops | bytes accessed | tf_op | source)
XLA Modules:
  0.0 217.6 jit_solution(1672351158851041666)
XLA Ops:
  0.6 212.1 %shard_map.112 = (bf16[1024,256]{1,0:T(8,128)(2,1)}, bf16[320,2048]{1,0:T(8,128)(2,1)}, f32[32,256]{1,0:T(8,128)}) custom-call(bf16[1280,2048]{1,0:T(8,128)(2,1)} %store_hbm.1, bf16[2048,256]{1,0:T(8,128)(2,1)} %wk_hbm.1, bf16[2048,256]{1,0:T(8,128)(2,1)} %wv_hbm.1, bf16[1024,256]{1,0:T(8,128)(2,1)} %q_hbm.1, bf16[1024,256]{1,0:T(8,128)(2,1)} %gate_hbm.1, ...), custom_call_target="tpu_custom_call" | custom-call | tf_op jit(solution)/shard_map/pallas_call | solution.py:551
  212.7 0.0 copy-start
  212.7 0.0 copy-start.1
  212.7 3.2 %convert_element_type.7 = f32[320,2048]{1,0:T(8,128)} convert(bf16[320,2048]{1,0:T(8,128)(2,1)} %get-tuple-element.7) | non-fusion elementwise | flops 655360 | bytes 3932160 | tf_op jit(solution)/shard_map/convert_element_type | solution.py:624
  215.9 0.0 copy-done
  215.9 1.0 convert_element_type.6
  217.0 0.0 copy-done.1
  217.0 0.6 copy.13
Async XLA Ops:
  212.7 3.2 %copy-start = (bf16[1024,256]{1,0:T(8,128)(2,1)S(1)}, bf16[1024,256]{1,0:T(8,128)(2,1)}, u32[]{:S(2)}) copy-start(bf16[1024,256]{1,0:T(8,128)(2,1)} %get-tuple-element.6) | copy-start | bytes 1572868
  212.7 4.2 %copy-start.1 = (f32[32,256]{1,0:T(8,128)S(1)}, f32[32,256]{1,0:T(8,128)}, u32[]{:S(2)}) copy-start(f32[32,256]{1,0:T(8,128)} %get-tuple-element.14) | copy-start | bytes 98308

commit v5 on v4

--- a/solution.py
+++ b/solution.py
@@ -528,6 +528,23 @@
     bulk_wait(wk_all, nx - 1, ssem.at[WK])
     bulk_wait(wv_all, nx - 1, ssem.at[WV])
     bulk_wait(own_v, nx - 1, ssem.at[XV])
+
+
+def widen_kernel(*refs):
+    half = len(refs) // 2
+    for src, dst in zip(refs[:half], refs[half:]):
+        dst[...] = src[...].astype(F32)
+
+
+def widened(arrays, steps):
+    specs = [pl.BlockSpec((a.shape[0] // steps, a.shape[1]), lambda i: (i, 0)) for a in arrays]
+    return pl.pallas_call(
+        widen_kernel,
+        grid=(steps,),
+        out_shape=tuple(jax.ShapeDtypeStruct(a.shape, F32) for a in arrays),
+        in_specs=specs,
+        out_specs=tuple(specs),
+    )(*arrays)
 
 
 def local(dims, queries, gate_pre, cotangent, store, store_gain, w_key, w_value, owners, slots):
@@ -621,7 +638,7 @@
         owners.T,
         slots.T,
     )
-    return dq.astype(F32), gs.astype(F32), gw
+    return widened((dq, gs, gw), 4)
 
 
 def solution(mesh):

time: 218 us -> 217 us (level)
  other arithmetic: 4.22 us -> 0 us
  Pallas kernels: 212 us -> 216 us
    convert_element_type x2 -> x0, other arithmetic: 4.22 us -> none  [local(): return (dq.astype(F32), gs.astype(F32), gw)]
    pallas_call x0 -> x1, Pallas kernels: none -> 4 us  [widened(): pl.pallas_call(widen_kernel, grid=(steps,), out_shape=tuple((jax.ShapeDty...]
where the time goes in v5:
time: 217 us
  Pallas kernels  216 us (100%)
    pallas_call x1, Pallas kernels, local(): pl.pallas_call(functools.partial(kernel, (nz, ny, nc, nx, npass)), out_sh...  212 us

profile of v5, /device:TPU:1, one launch (start us, length us, event | category | flops | bytes accessed | tf_op | source)
XLA Modules:
  0.0 216.7 jit_solution(18441077862110341185)
XLA Ops:
  0.6 212.1 %shard_map.112 = (bf16[1024,256]{1,0:T(8,128)(2,1)}, bf16[320,2048]{1,0:T(8,128)(2,1)}, f32[32,256]{1,0:T(8,128)}) custom-call(bf16[1280,2048]{1,0:T(8,128)(2,1)} %store_hbm.1, bf16[2048,256]{1,0:T(8,128)(2,1)} %wk_hbm.1, bf16[2048,256]{1,0:T(8,128)(2,1)} %wv_hbm.1, bf16[1024,256]{1,0:T(8,128)(2,1)} %q_hbm.1, bf16[1024,256]{1,0:T(8,128)(2,1)} %gate_hbm.1, ...), custom_call_target="tpu_custom_call" | custom-call | tf_op jit(solution)/shard_map/pallas_call | solution.py:568
  212.7 4.0 %shard_map.113 = (f32[1024,256]{1,0:T(8,128)}, f32[320,2048]{1,0:T(8,128)}, f32[32,256]{1,0:T(8,128)}) custom-call(bf16[1024,256]{1,0:T(8,128)(2,1)} %get-tuple-element.6.refs_0_, bf16[320,2048]{1,0:T(8,128)(2,1)} %get-tuple-element.7.refs_1_, f32[32,256]{1,0:T(8,128)} %get-tuple-element.8.refs_2_), custom_call_target="tpu_custom_call" | custom-call | tf_op jit(solution)/shard_map/pallas_call | solution.py:541
